TPU v7x, 32 devices: a whole 2x2x4 slice. The times are simulated.
32 devices in a mesh: grp: 2 (over y), sp: 4 (over z), tp: 4 (over x, core).
Axes of the slice: x: 2, y: 2, z: 4, core: 2. Of those that a mesh axis runs over, the one named last changes fastest.
Arguments:
- tokens: bfloat16 [4096, 2048], P(('grp', 'sp')), parts along dimension 0, may hold values from -6 to 6
- fresh_token_input: bfloat16 [4096], P('grp'), parts along dimension 0, may hold values from -6 to 6
- value_matrix: bfloat16 [2048, 2048], P(None, 'tp'), may hold values from -0.125 to 0.125
- write_matrix: bfloat16 [2048, 1024], P(None, 'tp'), may hold values from -0.125 to 0.125
- read_matrix: bfloat16 [2048, 1024], P(None, 'tp'), may hold values from -0.125 to 0.125
- gate_matrix: bfloat16 [2048, 2048], P(None, 'tp'), may hold values from -0.125 to 0.125
- step_matrix: bfloat16 [2048, 32], replicated, may hold values from -0.125 to 0.125
- value_filter_taps: bfloat16 [4, 2048], replicated, may hold values from -3 to 3
- write_filter_taps: bfloat16 [4, 1024], replicated, may hold values from -3 to 3
- read_filter_taps: bfloat16 [4, 1024], replicated, may hold values from -3 to 3
- head_log_decay: float32 [32], replicated
- step_offset_bias: float32 [32], replicated, may hold values from -3.5 to -2.5
- decay_spike: float32 [4096, 32], P(('grp', 'sp'), 'tp'), parts along dimension 0, may hold values from -3 to 0, as said below
- bypass_scale: float32 [32], replicated, may hold values from 0.5 to 2
- group_norm_scale: float32 [2048], replicated, may hold values from 0.1 to 1.9
Outputs:
- prompt_out: bfloat16 [4096, 2048], P(('grp', 'sp'), 'tp'), parts along dimension 0
- state_cache: bfloat16 [256, 2048], P(('grp', 'sp'), 'tp'), parts along dimension 0
- step_out: bfloat16 [1024, 4], P(('grp', 'tp'), 'sp'), parts along dimension 0
There are 2 independent parts, one for each index of `grp`. A program takes and returns all parts, laid end to end along the dimension named above; an argument that names none is the same for every part. Nothing has to cross between parts.
Inputs may be any that keep to these rules, and one draw needn't show every extreme that they name: `decay_spike`: never positive.
All inputs are finite; a program needn't handle non-finite values.
Results may differ from a plain program's by a relative error of at most 0.023.
Values may be sent and summed in bfloat16 or wider, within the bound.
A program may use at most 64 MiB of HBM per device.

v0:
```python
import jax
import jax.numpy as jnp
from jax import lax
from jax.sharding import PartitionSpec as P

HEAD = 64
STATE = 128
CONV = 4
BLOCK = 128
epsilon = 1e-06


def passed_along(block, axis, distance):
    devices = range(lax.axis_size(axis))
    route = [(i - distance, i) for i in devices if i - distance in devices]
    return lax.ppermute(block, axis, route)


def from_root(value, axis, source):
    kept = jnp.where(lax.axis_index(axis) == source, value, 0).astype(value.dtype)
    return lax.psum(kept, axis)


def project(operand, weights):
    return jnp.dot(operand, weights, preferred_element_type=jnp.float32).astype(jnp.bfloat16)


def apply_taps(previous, current, tap_weights):
    joined = jnp.concatenate([previous, current], axis=0).astype(jnp.float32)
    length = current.shape[0]
    summed = jnp.zeros(current.shape, jnp.float32)
    for offset in range(CONV):
        summed = summed + tap_weights[offset].astype(jnp.float32) * joined[offset : offset + length]
    return summed


def group_norm(gated_rows, groups):
    shaped = gated_rows.reshape(gated_rows.shape[:-1] + (groups, -1))
    normed = shaped * lax.rsqrt(jnp.mean(shaped * shaped, axis=-1, keepdims=True) + epsilon)
    return normed.reshape(gated_rows.shape)


def read_new(cached, stored_portion, read_part, new_decay, step_now, value_now):
    states = cached.astype(jnp.float32).reshape((cached.shape[0],) + value_now.shape)
    updated = (
        new_decay[None, :, :, None] * states
        + step_now[None, :, :, None] * stored_portion.T[:, :, None, None] * value_now[None]
    )
    return jnp.einsum("gn,ngep->gep", read_part, updated, precision=lax.Precision.HIGHEST)


def on_device(
    tokens,
    fresh_token_input,
    value_matrix,
    write_matrix,
    read_matrix,
    gate_matrix,
    step_matrix,
    value_filter_taps,
    write_filter_taps,
    read_filter_taps,
    head_log_decay,
    step_offset_bias,
    decay_spike,
    bypass_scale,
    group_norm_scale,
):
    head_rank = lax.axis_index("tp")
    sequence_rank = lax.axis_index("sp")
    sequence_count = lax.axis_size("sp")
    channels = value_matrix.shape[1]
    head_count = channels // HEAD
    map_width = write_matrix.shape[1]
    group_count = map_width // STATE
    per_group = head_count // group_count
    row_count = tokens.shape[0]
    head_start = head_rank * head_count
    local_count = STATE // sequence_count
    own_step = lax.dynamic_slice_in_dim(step_matrix, head_start, head_count, 1)
    own_value_taps = lax.dynamic_slice_in_dim(value_filter_taps, head_rank * channels, channels, 1)
    own_write_taps = lax.dynamic_slice_in_dim(
        write_filter_taps, head_rank * map_width, map_width, 1
    )
    own_read_taps = lax.dynamic_slice_in_dim(read_filter_taps, head_rank * map_width, map_width, 1)
    head_decay_rates = jnp.exp(lax.dynamic_slice_in_dim(head_log_decay, head_start, head_count, 0))
    own_bias = lax.dynamic_slice_in_dim(step_offset_bias, head_start, head_count, 0)
    own_skip = lax.dynamic_slice_in_dim(bypass_scale, head_start, head_count, 0)
    own_gain = lax.dynamic_slice_in_dim(group_norm_scale, head_rank * channels, channels, 0)
    value_rows = project(tokens, value_matrix)
    write_rows = project(tokens, write_matrix)
    read_rows = project(tokens, read_matrix)
    gate_rows = project(tokens, gate_matrix)
    step_raw = jnp.dot(tokens, own_step, preferred_element_type=jnp.float32)
    edge = row_count - (CONV - 1)
    tail_rows = (value_rows[edge:], write_rows[edge:], read_rows[edge:])
    before = passed_along((tail_rows[0], tail_rows[1], tail_rows[2]), "sp", 1)
    ending = (
        from_root(tail_rows[0], "sp", sequence_count - 1),
        from_root(tail_rows[1], "sp", sequence_count - 1),
        from_root(tail_rows[2], "sp", sequence_count - 1),
    )
    values = jax.nn.silu(apply_taps(before[0], value_rows, own_value_taps)).astype(jnp.bfloat16)
    writes = jax.nn.silu(apply_taps(before[1], write_rows, own_write_taps)).astype(jnp.bfloat16)
    reads = jax.nn.silu(apply_taps(before[2], read_rows, own_read_taps)).astype(jnp.bfloat16)
    step_length = jax.nn.softplus(step_raw + own_bias)
    log_decay_value = decay_spike - step_length * head_decay_rates
    blocks = row_count // BLOCK
    block_values = values.reshape(blocks, BLOCK, group_count, per_group, HEAD)
    block_writes = writes.reshape(blocks, BLOCK, group_count, STATE)
    block_reads = reads.reshape(blocks, BLOCK, group_count, STATE)
    block_steps = step_length.reshape(blocks, BLOCK, group_count, per_group)
    cumulative = jnp.cumsum(log_decay_value.reshape(blocks, BLOCK, group_count, per_group), axis=1)
    block_end = cumulative[:, -1]
    scaled = (
        (jnp.exp(block_end[:, None] - cumulative) * block_steps)[..., None]
        * block_values.astype(jnp.float32)
    ).astype(jnp.bfloat16)
    block_states = jnp.einsum(
        "bsgn,bsgep->bngep", block_writes, scaled, preferred_element_type=jnp.float32
    )
    running = jnp.zeros((STATE, group_count, per_group, HEAD), jnp.float32)
    inside = []
    for block_index in range(blocks):
        inside.append(running)
        running = (
            jnp.exp(block_end[block_index])[None, :, :, None] * running + block_states[block_index]
        )
    local_states = jnp.stack(inside)
    shard_fading_factor = jnp.sum(block_end, axis=0)
    before_block = jnp.cumsum(block_end, axis=0) - block_end
    decay_table = lax.all_gather(shard_fading_factor[None], "sp", axis=0, tiled=True)
    inclusive = jnp.cumsum(decay_table, axis=0)
    exclusive = inclusive - decay_table
    total_decay = inclusive[-1]
    row_pieces = lax.all_to_all(running[None], "sp", split_axis=1, concat_axis=0, tiled=True)
    ranks = jnp.arange(sequence_count)
    below = (ranks[None, :] < ranks[:, None])[:, :, None, None]
    prefix_weight = jnp.exp(jnp.where(below, exclusive[:, None] - inclusive[None, :], -jnp.inf))
    prefix_rows = jnp.einsum(
        "jkge,kngep->jngep", prefix_weight, row_pieces, precision=lax.Precision.HIGHEST
    )
    final_weight = jnp.exp(total_decay[None] - inclusive)
    final_rows = jnp.einsum(
        "kge,kngep->ngep", final_weight, row_pieces, precision=lax.Precision.HIGHEST
    )
    earlier_state = lax.all_to_all(prefix_rows, "sp", split_axis=0, concat_axis=1, tiled=True)[0]
    scores = jnp.einsum(
        "blgn,bsgn->bgls", block_reads, block_writes, preferred_element_type=jnp.float32
    )
    cum_heads = jnp.transpose(cumulative, (0, 2, 3, 1))
    decay_gaps = cum_heads[..., :, None] - cum_heads[..., None, :]
    step_heads = jnp.transpose(block_steps, (0, 2, 3, 1))
    causal = jnp.tril(jnp.ones((BLOCK, BLOCK), bool))
    mixing = (
        scores[:, :, None]
        * jnp.exp(jnp.where(causal, decay_gaps, -jnp.inf))
        * step_heads[..., None, :]
    ).astype(jnp.bfloat16)
    inner_part = jnp.einsum(
        "bgels,bsgep->blgep", mixing, block_values, preferred_element_type=jnp.float32
    )
    entering = jnp.exp(before_block)[:, None, :, :, None] * earlier_state[None] + local_states
    carried_part = jnp.exp(cumulative)[..., None] * jnp.einsum(
        "blgn,bngep->blgep",
        block_reads.astype(jnp.float32),
        entering,
        precision=lax.Precision.HIGHEST,
    )
    mixed_rows = (inner_part + carried_part).reshape(row_count, head_count, HEAD) + own_skip[
        None, :, None
    ] * values.astype(jnp.float32).reshape(row_count, head_count, HEAD)
    gated_rows = mixed_rows.reshape(row_count, channels) * jax.nn.silu(
        gate_rows.astype(jnp.float32)
    )
    prompt_out = (group_norm(gated_rows, group_count) * own_gain).astype(jnp.bfloat16)
    new_row = fresh_token_input[None]
    new_value = project(new_row, value_matrix)
    new_write = project(new_row, write_matrix)
    new_read = project(new_row, read_matrix)
    new_gate = project(new_row, gate_matrix)
    new_step = jax.nn.softplus(
        jnp.dot(new_row, own_step, preferred_element_type=jnp.float32)[0] + own_bias
    )
    new_values = jax.nn.silu(apply_taps(ending[0], new_value, own_value_taps)).astype(jnp.bfloat16)
    latest_stores = jax.nn.silu(apply_taps(ending[1], new_write, own_write_taps)).astype(
        jnp.bfloat16
    )
    new_reads = jax.nn.silu(apply_taps(ending[2], new_read, own_read_taps)).astype(jnp.bfloat16)
    value_now = new_values.astype(jnp.float32).reshape(group_count, per_group, HEAD)
    write_now = latest_stores.astype(jnp.float32).reshape(group_count, STATE)
    read_now = new_reads.astype(jnp.float32).reshape(group_count, STATE)
    new_decay = jnp.exp(-new_step * head_decay_rates).reshape(group_count, per_group)
    step_now = new_step.reshape(group_count, per_group)
    row_start = sequence_rank * local_count
    cache_rows = final_rows.reshape(local_count, channels).astype(jnp.bfloat16)
    stored_portion = lax.dynamic_slice_in_dim(write_now, row_start, local_count, 1)
    read_part = lax.dynamic_slice_in_dim(read_now, row_start, local_count, 1)
    partial_value = read_new(cache_rows, stored_portion, read_part, new_decay, step_now, value_now)
    reading = lax.psum(partial_value, "sp")
    new_mixed = reading + own_skip.reshape(group_count, per_group)[:, :, None] * value_now
    new_gated = new_mixed.reshape(1, channels) * jax.nn.silu(new_gate.astype(jnp.float32))
    step_whole = (group_norm(new_gated, group_count) * own_gain).astype(jnp.bfloat16)[0]
    step_table = step_whole.reshape(channels // sequence_count, sequence_count)
    step_out = lax.dynamic_slice_in_dim(step_table, sequence_rank, 1, 1)
    return (prompt_out, cache_rows, step_out)


def solution(mesh):
    placed = (
        P(("grp", "sp"), None),
        P("grp"),
        P(None, "tp"),
        P(None, "tp"),
        P(None, "tp"),
        P(None, "tp"),
        P(),
        P(),
        P(),
        P(),
        P(),
        P(),
        P(("grp", "sp"), "tp"),
        P(),
        P(),
    )
    return jax.shard_map(
        on_device,
        mesh=mesh,
        in_specs=placed,
        out_specs=(P(("grp", "sp"), "tp"), P(("grp", "sp"), "tp"), P(("grp", "tp"), "sp")),
        check_vma=False,
    )
```

profile of v0, /device:TPU:0, one launch (start us, length us, event | category | flops | bytes accessed | tf_op | source)
XLA Modules:
  0.0 126.4 jit_solution(4960432107386798171)
XLA Ops:
  0.7 1.6 %copy-done = bf16[512,2048]{1,0:T(8,128)(2,1)S(1)} copy-done((bf16[512,2048]{1,0:T(8,128)(2,1)S(1)}, bf16[512,2048]{1,0:T(8,128)(2,1)}, u32[]{:S(2)}) %copy-start) | copy-done | bytes 2097176
  2.2 1.9 %convolution_convert_fusion.2 = bf16[512,256]{1,0:T(8,128)(2,1)S(1)} fusion(bf16[512,2048]{1,0:T(8,128)(2,1)S(1)} %copy-done, bf16[2048,256]{1,0:T(8,128)(2,1)} %param.18), kind=kOutput, calls=%fused_computation.11 | convolution fusion | flops 537001984 | bytes 3407872 | tf_op jit(solution)/shard_map/dot_general | solution.py:25
  4.7 5.7 %collective-permute-start.2 = (bf16[3,256]{1,0:T(4,128)(2,1)}, bf16[3,256]{1,0:T(4,128)(2,1)}, u32[]{:S(2)}, u32[]{:S(2)}) collective-permute-start(bf16[3,256]{1,0:T(4,128)(2,1)} %get-tuple-element.57), channel_id=1, source_target_pairs={{0,4},{4,8},{8,12},{1,5},{5,9},{9,13},{2,6},{6,10},{10,14},{3,7},{... | collective-permute-start | bytes 4616 | tf_op jit(solution)/shard_map/ppermute | solution.py:16
  10.4 0.7 convolution_convert_fusion.3
  11.8 3.6 %collective-permute-start.1 = (bf16[3,256]{1,0:T(4,128)(2,1)}, bf16[3,256]{1,0:T(4,128)(2,1)}, u32[]{:S(2)}, u32[]{:S(2)}) collective-permute-start(bf16[3,256]{1,0:T(4,128)(2,1)} %get-tuple-element.54), channel_id=1, source_target_pairs={{0,4},{4,8},{8,12},{1,5},{5,9},{9,13},{2,6},{6,10},{10,14},{3,7},{... | collective-permute-start | bytes 4616 | tf_op jit(solution)/shard_map/ppermute | solution.py:16
  15.4 1.3 convolution_convert_fusion.1
  16.7 0.8 copy-done.8
  18.1 3.5 %collective-permute-start = (bf16[3,512]{1,0:T(4,128)(2,1)}, bf16[3,512]{1,0:T(4,128)(2,1)}, u32[]{:S(2)}, u32[]{:S(2)}) collective-permute-start(bf16[3,512]{1,0:T(4,128)(2,1)} %get-tuple-element.52), channel_id=1, source_target_pairs={{0,4},{4,8},{8,12},{1,5},{5,9},{9,13},{2,6},{6,10},{10,14},{3,7},{... | collective-permute-start | bytes 9224 | tf_op jit(solution)/shard_map/ppermute | solution.py:16
  22.4 1.5 %fusion.96 = f32[1,256]{1,0:T(1,128)S(1)} fusion(bf16[2048,1]{0,1:T(2,128)(2,1)S(1)} %reshape.251, bf16[2048,256]{1,0:T(8,128)(2,1)} %param.19), kind=kOutput, calls=%fused_computation.194 | convolution fusion | flops 1048576 | bytes 1053696 | tf_op jit(solution)/shard_map/dot_general | solution.py:25
  27.1 2.0 %fusion.99 = f32[1,512]{1,0:T(1,128)S(1)} fusion(bf16[2048,1]{0,1:T(2,128)(2,1)S(1)} %reshape.251, bf16[2048,512]{1,0:T(8,128)(2,1)} %param.20), kind=kOutput, calls=%fused_computation.197 | convolution fusion | flops 2097152 | bytes 2103296 | tf_op jit(solution)/shard_map/dot_general | solution.py:25
  29.1 7.6 %all-gather.1 = f32[4,2,4]{2,1,0:T(2,128)S(1)} all-gather(f32[1,2,4]{2,1,0:T(2,128)S(1)} %bitcast.152), channel_id=2, replica_groups=mesh['grp'=2,'sp'=4,'tp'=4] {'sp'}, dimensions={0}, use_global_device_ids=true | all-gather | bytes 160 | tf_op jit(solution)/shard_map/all_gather | solution.py:132
  36.7 10.5 %all-reduce = (bf16[3,512]{1,0:T(4,128)(2,1)S(1)}, bf16[3,256]{1,0:T(4,128)(2,1)S(1)}, bf16[3,256]{1,0:T(4,128)(2,1)S(1)}) all-reduce(bf16[3,512]{1,0:T(4,128)(2,1)S(1)} %get-tuple-element.53, bf16[3,256]{1,0:T(4,128)(2,1)S(1)} %get-tuple-element.56, ...), channel_id=1, replica_groups=mesh['grp'=2,'sp'=4,'tp'=4] {'sp'}, use_global_device_ids=true, to_apply=%region_7.8 | all-reduce | flops 3072 | bytes 12288 | tf_op jit(solution)/shard_map/psum | solution.py:21
  48.1 1.0 copy.149
  49.2 0.7 convert_reduce_fusion.1
  49.9 2.4 %fusion.90 = (f32[4,128,2,4]{3,2,1,0:T(2,128)}, f32[4,128,2,4]{3,2,1,0:T(2,128)S(1)}) fusion(f32[4,128,2,4]{3,2,1,0:T(2,128)S(1)} %fusion.94, f32[4,128,2,4]{3,2,1,0:T(2,128)} %copy.149, f32[4,2,4]{2,1,0:T(2,128)S(1)} %get-tuple-element.47), kind=kLoop, calls=%fused_computation.187 | loop fusion | flops 8192 | bytes 65664 | tf_op jit(solution)/shard_map/exp | solution.py:164
  52.4 0.7 convert_reduce_fusion
  53.7 0.7 dynamic_slice.39
  55.9 1.3 %mul.529 = f32[2,4]{1,0:T(2,128)} reshape(f32[8]{0:T(128)} %get-tuple-element.28) | data formatting | bytes 64 | tf_op jit(solution)/shard_map/mul | solution.py:46
  57.6 1.3 %copy.148 = f32[4,128,2,4]{1,3,2,0:T(4,128)S(1)} copy(f32[4,128,2,4]{3,2,1,0:T(2,128)} %get-tuple-element.44) | data formatting | bytes 32768 | tf_op jit(solution)/shard_map/exp | solution.py:164
  59.7 0.7 maximum_convert_fusion.2
  60.5 1.0 multiply_convert_fusion.5
  61.5 0.8 maximum_convert_fusion.1
  62.8 0.8 maximum_convert_fusion
  63.6 1.3 %multiply_convert_fusion.4 = bf16[512,512]{1,0:T(8,128)(2,1)S(1)} fusion(f32[515,512]{1,0:T(8,128)S(1)} %maximum_convert_fusion, f32[512]{0:T(512)} %bitcast.141, f32[512]{0:T(512)} %bitcast.140, f32[512]{0:T(512)S(1)} %bitcast.139, f32[512]{0:T(512)S(1)} %bitcast.138), kind=kLoop, calls=%fused_computation.44 | loop fusion | flops 3145728 | bytes 4726784 | tf_op jit(solution)/shard_map/convert_element_type | solution.py:103
  65.0 1.0 copy.140
  66.0 2.0 %reshape.229 = bf16[4,128,2,4,64]{1,0,4,3,2:T(4,128)(2,1)} reshape(bf16[512,512]{0,1:T(8,128)(2,1)} %copy.140) | data formatting | bytes 1048576 | tf_op jit(solution)/shard_map/reshape | solution.py:109
  68.0 1.3 multiply_convert_fusion.3
  69.5 1.0 slice_add_fusion
  70.8 1.2 reshape.274
  72.0 3.6 %all-to-all-start = ((f32[4,1,16384]{2,1,0:T(1,128)}), f32[4,1,16384]{2,1,0:T(1,128)S(1)}, u32[]{:S(2)}, u32[]{:S(2)}) async-start(f32[4,1,16384]{2,1,0:T(1,128)} %reshape.274), calls=%async_computation | async-start | bytes 524288 | tf_op jit(solution)/shard_map/all_to_all | solution.py:136
  75.9 3.0 %convolution_bitcast_fusion.2 = f32[4,128,2,4,64]{1,4,3,2,0:T(8,128)} fusion(f32[4,2,4,128]{3,2,1,0:T(4,128)S(1)} %copy.146, f32[4,2,4,128]{3,2,1,0:T(4,128)S(1)} %copy.144, f32[4,2,128,128]{3,2,1,0:T(8,128)S(1)} %fusion.40, pred[128,128]{1,0:T(8,128)(4,1)S(1)} %iota_compare_fusion, bf16[4,128,2,4,64]{1,0,4,3,2:T(4,128)(2,1)} %reshape.229), kind=kOutput, calls=%fused_computation.5 | convolution fusion | flops 69730304 | bytes 2146304 | tf_op jit(solution)/shard_map/bgels,bsgep->blgep/dot_general | solution.py:160
  78.8 3.3 %all-to-all-done = f32[4,1,16384]{2,1,0:T(1,128)S(1)} async-done(((f32[4,1,16384]{2,1,0:T(1,128)}), f32[4,1,16384]{2,1,0:T(1,128)S(1)}, u32[]{:S(2)}, u32[]{:S(2)}) %all-to-all-start) | async-done | bytes 262176 | tf_op jit(solution)/shard_map/all_to_all | solution.py:136
  82.7 1.3 %reduce.9 = f32[4,16384]{1,0:T(4,128)S(1)} reduce(f32[4,1,16384]{2,1,0:T(1,128)S(1)} %all-to-all-done, f32[]{:T(128)} %broadcast.118), dimensions={1}, to_apply=%all_to_all.6.reduce_sub_computation | reduce | bytes 524292 | tf_op jit(solution)/shard_map/all_to_all | solution.py:136
  84.4 1.3 %fusion.35 = bf16[2,4,1,32,64]{4,2,3,1,0:T(2,128)(2,1)S(1)} fusion(f32[4,2,4,1,1]{0,3,4,2,1:T(1,128)S(1)} %copy.173, f32[4,32,2,4,64]{4,3,2,1,0:T(4,128)S(1)} %bitcast.123), kind=kOutput, calls=%fused_computation.69 | convolution fusion | flops 786432 | bytes 295040 | tf_op jit(solution)/shard_map/kge,kngep->ngep/dot_general | solution.py:144
  85.7 1.3 %convolution_bitcast_fusion.3 = f32[4,32,2,4,64]{4,0,1,3,2:T(4,128)S(1)} fusion(f32[4,32,2,4,64]{4,3,2,1,0:T(4,128)S(1)} %bitcast.124, f32[4,2,4]{0,2,1:T(4,128)S(1)} %copy.156, f32[4,2,4]{0,2,1:T(4,128)S(1)} %copy.155, pred[4,4]{1,0:T(4,128)(4,1)S(1)} %copy-done.30), kind=kOutput, calls=%fused_computation.10 | convolution fusion | flops 3145984 | bytes 524560 | tf_op jit(solution)/shard_map/jkge,kngep->jngep/dot_general | solution.py:140
  87.1 1.0 reshape.276
  88.1 3.4 %all-to-all-start.1 = ((f32[4,1,16384]{2,1,0:T(1,128)}), f32[4,1,16384]{2,1,0:T(1,128)S(1)}, u32[]{:S(2)}, u32[]{:S(2)}) async-start(f32[4,1,16384]{2,1,0:T(1,128)} %reshape.276), calls=%async_computation.1 | async-start | bytes 524288 | tf_op jit(solution)/shard_map/all_to_all | solution.py:147
  91.9 12.2 %psum.31 = f32[2,4,64]{2,1,0:T(4,128)S(1)} all-reduce(f32[2,4,64]{2,1,0:T(4,128)S(1)} %bitcast.137), channel_id=1, replica_groups=mesh['grp'=2,'sp'=4,'tp'=4] {'sp'}, use_global_device_ids=true, to_apply=%region_8.9 | all-reduce | flops 512 | bytes 4096 | tf_op jit(solution)/shard_map/psum | solution.py:200
  104.5 0.7 convert_element_type.211
  105.3 0.8 multiply_convert_fusion.7
  106.9 1.3 %reduce.10 = f32[4,16384]{1,0:T(4,128)S(1)} reduce(f32[4,1,16384]{2,1,0:T(1,128)S(1)} %all-to-all-done.1, f32[]{:T(128)} %broadcast.118), dimensions={1}, to_apply=%all_to_all.8.reduce_sub_computation | reduce | bytes 524292 | tf_op jit(solution)/shard_map/all_to_all | solution.py:147
  108.5 0.9 copy.160
  109.4 2.3 %fusion.1 = f32[4,128,2,4,64]{1,4,3,2,0:T(8,128)S(1)} fusion(f32[4,128,2,4,64]{1,4,3,2,0:T(8,128)} %convolution_bitcast_fusion.2, f32[1,128,2,4,64]{1,4,3,2,0:T(8,128)} %get-tuple-element.41, f32[1,128,2,4,64]{1,4,3,2,0:T(8,128)} %get-tuple-element.42, f32[1,128,2,4,64]{1,4,3,2,0:T(8,128)} %get-tuple-element.43, f32[4]{0:T(128)S(1)} %copy-done.31, ...), kind=kOutput, calls=%fused_computation.4 | convolution fusion | flops 404488192 | bytes 3424400 | tf_op jit(solution)/shard_map/blgn,bngep->blgep/dot_general | solution.py:164
  111.7 1.8 %copy.184 = f32[4,128,2,4,64]{4,3,2,1,0:T(4,128)} copy(f32[4,128,2,4,64]{1,4,3,2,0:T(8,128)S(1)} %fusion.1) | data formatting | bytes 2097152 | tf_op jit(solution)/shard_map/reshape | solution.py:170
  113.5 3.5 %reshape.263 = f32[512,512]{1,0:T(8,128)} reshape(f32[4,128,2,4,64]{4,3,2,1,0:T(4,128)} %copy.184) | data formatting | bytes 2097152 | tf_op jit(solution)/shard_map/reshape | solution.py:170
  117.0 4.6 %fusion.93 = (f32[512,512]{1,0:T(8,128)}, f32[512,512]{1,0:T(8,128)}) fusion(bf16[512,2048]{1,0:T(8,128)(2,1)S(1)} %copy-done, bf16[2048,512]{1,0:T(8,128)(2,1)} %param.20, f32[512,512]{1,0:T(8,128)} %reshape.263, bf16[512,512]{1,0:T(8,128)(2,1)S(1)} %copy-done.2, f32[512]{0:T(512)S(1)} %copy-done.25), kind=kOutput, calls=%fused_computation.190 | convolution fusion | flops 1076625408 | bytes 7866368 | tf_op jit(solution)/shard_map/dot_general | solution.py:25
  121.7 1.9 %mul.516 = f32[512,2,256]{2,1,0:T(2,128)S(1)} reshape(f32[512,512]{1,0:T(8,128)} %get-tuple-element.63) | data formatting | bytes 2097152 | tf_op jit(solution)/shard_map/mul | solution.py:39
  125.4 1.1 multiply_convert_fusion.2
  (144 shorter events, 16.2 us)
Async XLA Ops:
  0.6 1.6 %copy-start = (bf16[512,2048]{1,0:T(8,128)(2,1)S(1)}, bf16[512,2048]{1,0:T(8,128)(2,1)}, u32[]{:S(2)}) copy-start(bf16[512,2048]{1,0:T(8,128)(2,1)} %param.15) | copy-start | bytes 6291460
  0.6 9.8 %copy-start.6 = (bf16[2048,256]{1,0:T(8,128)(2,1)S(1)}, bf16[2048,256]{1,0:T(8,128)(2,1)}, u32[]{:S(2)}) copy-start(bf16[2048,256]{1,0:T(8,128)(2,1)} %param.19) | copy-start | bytes 3145732
  4.2 11.3 %copy-start.3 = (bf16[2048,512]{1,0:T(8,128)(2,1)S(1)}, bf16[2048,512]{1,0:T(8,128)(2,1)}, u32[]{:S(2)}) copy-start(bf16[2048,512]{1,0:T(8,128)(2,1)} %param.17) | copy-start | bytes 6291460
  4.7 55.0 %collective-permute-start.2 = (bf16[3,256]{1,0:T(4,128)(2,1)}, bf16[3,256]{1,0:T(4,128)(2,1)}, u32[]{:S(2)}, u32[]{:S(2)}) collective-permute-start(bf16[3,256]{1,0:T(4,128)(2,1)} %get-tuple-element.57), channel_id=1, source_target_pairs={{0,4},{4,8},{8,12},{1,5},{5,9},{9,13},{2,6},{6,10},{10,14},{3,7},{... | collective-permute-start | bytes 4616 | tf_op jit(solution)/shard_map/ppermute | solution.py:16
  11.1 0.7 copy-start.10
  11.8 10.3 %copy-start.23 = (bf16[2048]{0:T(1024)(128)(2,1)S(1)}, bf16[2048]{0:T(1024)(128)(2,1)}, u32[]{:S(2)}) copy-start(bf16[2048]{0:T(1024)(128)(2,1)} %param.16) | copy-start | bytes 12292
  11.8 10.3 %copy-start.5 = (bf16[2048,256]{1,0:T(8,128)(2,1)S(1)}, bf16[2048,256]{1,0:T(8,128)(2,1)}, u32[]{:S(2)}) copy-start(bf16[2048,256]{1,0:T(8,128)(2,1)} %param.18) | copy-start | bytes 3145732
  11.8 49.6 %collective-permute-start.1 = (bf16[3,256]{1,0:T(4,128)(2,1)}, bf16[3,256]{1,0:T(4,128)(2,1)}, u32[]{:S(2)}, u32[]{:S(2)}) collective-permute-start(bf16[3,256]{1,0:T(4,128)(2,1)} %get-tuple-element.54), channel_id=1, source_target_pairs={{0,4},{4,8},{8,12},{1,5},{5,9},{9,13},{2,6},{6,10},{10,14},{3,7},{... | collective-permute-start | bytes 4616 | tf_op jit(solution)/shard_map/ppermute | solution.py:16
  16.7 0.8 copy-start.8
  18.1 44.7 %collective-permute-start = (bf16[3,512]{1,0:T(4,128)(2,1)}, bf16[3,512]{1,0:T(4,128)(2,1)}, u32[]{:S(2)}, u32[]{:S(2)}) collective-permute-start(bf16[3,512]{1,0:T(4,128)(2,1)} %get-tuple-element.52), channel_id=1, source_target_pairs={{0,4},{4,8},{8,12},{1,5},{5,9},{9,13},{2,6},{6,10},{10,14},{3,7},{... | collective-permute-start | bytes 9224 | tf_op jit(solution)/shard_map/ppermute | solution.py:16
  21.6 2.3 %copy-start.4 = (bf16[2048,512]{1,0:T(8,128)(2,1)S(1)}, bf16[2048,512]{1,0:T(8,128)(2,1)}, u32[]{:S(2)}) copy-start(bf16[2048,512]{1,0:T(8,128)(2,1)} %param.17) | copy-start | bytes 6291460
  22.1 2.2 %copy-start.33 = (f32[32]{0:T(128)S(1)}, f32[32]{0:T(128)}, u32[]{:S(2)}) copy-start(f32[32]{0:T(128)} %param.26) | copy-start | bytes 388
  22.2 2.3 %copy-start.32 = (f32[32]{0:T(128)S(1)}, f32[32]{0:T(128)}, u32[]{:S(2)}) copy-start(f32[32]{0:T(128)} %param.25) | copy-start | bytes 388
  22.2 3.0 %copy-start.12 = (f32[512,8]{0,1:T(8,128)S(1)}, f32[512,8]{0,1:T(8,128)}, u32[]{:S(2)}) copy-start(f32[512,8]{0,1:T(8,128)} %param.27) | copy-start | bytes 49156
  22.4 2.0 %copy-start.13 = (bf16[2048,32]{0,1:T(8,128)(2,1)S(1)}, bf16[2048,32]{0,1:T(8,128)(2,1)}, u32[]{:S(2)}) copy-start(bf16[2048,32]{0,1:T(8,128)(2,1)} %param.21) | copy-start | bytes 393220
  25.8 21.5 %copy-start.26 = (bf16[4,1024]{1,0:T(4,128)(2,1)S(1)}, bf16[4,1024]{1,0:T(4,128)(2,1)}, u32[]{:S(2)}) copy-start(bf16[4,1024]{1,0:T(4,128)(2,1)} %param.23) | copy-start | bytes 24580
  26.1 23.0 %copy-start.27 = (bf16[4,1024]{1,0:T(4,128)(2,1)S(1)}, bf16[4,1024]{1,0:T(4,128)(2,1)}, u32[]{:S(2)}) copy-start(bf16[4,1024]{1,0:T(4,128)(2,1)} %param.24) | copy-start | bytes 24580
  27.1 25.3 %copy-start.22 = (bf16[4,2048]{1,0:T(4,128)(2,1)S(1)}, bf16[4,2048]{1,0:T(4,128)(2,1)}, u32[]{:S(2)}) copy-start(bf16[4,2048]{1,0:T(4,128)(2,1)} %param.22) | copy-start | bytes 49156
  57.6 3.9 %copy-start.11 = (bf16[512,256]{1,0:T(8,128)(2,1)S(1)}, bf16[512,256]{1,0:T(8,128)(2,1)}, u32[]{:S(2)}) copy-start(bf16[512,256]{1,0:T(8,128)(2,1)} %copy-done.10) | copy-start | bytes 786436
  59.1 3.1 %copy-start.18 = (f32[1,256]{1,0:T(1,128)S(1)}, f32[1,256]{1,0:T(1,128)}, u32[]{:S(2)}) copy-start(f32[1,256]{1,0:T(1,128)} %get-tuple-element.24) | copy-start | bytes 3076
  59.1 3.2 %copy-start.19 = (f32[1,256]{1,0:T(1,128)S(1)}, f32[1,256]{1,0:T(1,128)}, u32[]{:S(2)}) copy-start(f32[1,256]{1,0:T(1,128)} %get-tuple-element.25) | copy-start | bytes 3076
  59.1 3.2 %copy-start.20 = (f32[1,256]{1,0:T(1,128)S(1)}, f32[1,256]{1,0:T(1,128)}, u32[]{:S(2)}) copy-start(f32[1,256]{1,0:T(1,128)} %get-tuple-element.26) | copy-start | bytes 3076
  59.1 3.2 %copy-start.21 = (f32[1,256]{1,0:T(1,128)S(1)}, f32[1,256]{1,0:T(1,128)}, u32[]{:S(2)}) copy-start(f32[1,256]{1,0:T(1,128)} %get-tuple-element.27) | copy-start | bytes 3076
  61.5 1.3 %copy-start.9 = (bf16[512,512]{1,0:T(8,128)(2,1)S(1)}, bf16[512,512]{1,0:T(8,128)(2,1)}, u32[]{:S(2)}) copy-start(bf16[512,512]{1,0:T(8,128)(2,1)} %copy-done.8) | copy-start | bytes 1572868
  65.0 4.5 %copy-start.1 = (bf16[512,512]{1,0:T(8,128)(2,1)}, bf16[512,512]{1,0:T(8,128)(2,1)S(1)}, u32[]{:S(2)}) copy-start(bf16[512,512]{1,0:T(8,128)(2,1)S(1)} %multiply_convert_fusion.4) | copy-start | bytes 1572868
  66.0 3.5 %copy-start.14 = (f32[2,4]{1,0:T(2,128)S(1)}, f32[2,4]{1,0:T(2,128)}, u32[]{:S(2)}) copy-start(f32[2,4]{1,0:T(2,128)} %get-tuple-element.48) | copy-start | bytes 100
  66.0 3.5 %copy-start.15 = (f32[2,4]{1,0:T(2,128)S(1)}, f32[2,4]{1,0:T(2,128)}, u32[]{:S(2)}) copy-start(f32[2,4]{1,0:T(2,128)} %get-tuple-element.49) | copy-start | bytes 100
  68.0 1.6 %copy-start.16 = (f32[2,4]{1,0:T(2,128)S(1)}, f32[2,4]{1,0:T(2,128)}, u32[]{:S(2)}) copy-start(f32[2,4]{1,0:T(2,128)} %get-tuple-element.50) | copy-start | bytes 100
  68.0 1.6 %copy-start.17 = (f32[2,4]{1,0:T(2,128)S(1)}, f32[2,4]{1,0:T(2,128)}, u32[]{:S(2)}) copy-start(f32[2,4]{1,0:T(2,128)} %get-tuple-element.51) | copy-start | bytes 100
  72.0 10.2 %all-to-all-start = ((f32[4,1,16384]{2,1,0:T(1,128)}), f32[4,1,16384]{2,1,0:T(1,128)S(1)}, u32[]{:S(2)}, u32[]{:S(2)}) async-start(f32[4,1,16384]{2,1,0:T(1,128)} %reshape.274), calls=%async_computation | async-start | bytes 524288 | tf_op jit(solution)/shard_map/all_to_all | solution.py:136
  75.9 9.8 %copy-start.30 = (pred[4,4]{1,0:T(4,128)(4,1)S(1)}, pred[4,4]{1,0:T(4,128)(4,1)}, u32[]{:S(2)}) copy-start(pred[4,4]{1,0:T(4,128)(4,1)} %iota_compare_fusion.1) | copy-start | bytes 52
  84.3 7.2 %copy-start.28 = (f32[2,4]{1,0:T(2,128)S(1)}, f32[2,4]{1,0:T(2,128)}, u32[]{:S(2)}) copy-start(f32[2,4]{1,0:T(2,128)} %mul.529) | copy-start | bytes 100
  84.3 7.4 %copy-start.24 = (bf16[2,32,1,1]{1,0,2,3:T(2,128)(2,1)S(1)}, bf16[2,32,1,1]{1,0,2,3:T(2,128)(2,1)}, u32[]{:S(2)}) copy-start(bf16[2,32,1,1]{1,0,2,3:T(2,128)(2,1)} %fusion.81) | copy-start | bytes 388
  85.7 18.4 %copy-start.29 = (f32[2,4]{1,0:T(2,128)S(1)}, f32[2,4]{1,0:T(2,128)}, u32[]{:S(2)}) copy-start(f32[2,4]{1,0:T(2,128)} %mul.552) | copy-start | bytes 100
  88.1 18.8 %all-to-all-start.1 = ((f32[4,1,16384]{2,1,0:T(1,128)}), f32[4,1,16384]{2,1,0:T(1,128)S(1)}, u32[]{:S(2)}, u32[]{:S(2)}) async-start(f32[4,1,16384]{2,1,0:T(1,128)} %reshape.276), calls=%async_computation.1 | async-start | bytes 524288 | tf_op jit(solution)/shard_map/all_to_all | solution.py:147
  91.5 17.9 %copy-start.31 = (f32[4]{0:T(128)S(1)}, f32[4]{0:T(128)}, u32[]{:S(2)}) copy-start(f32[4]{0:T(128)} %pad.6.clone) | copy-start | bytes 52
  113.5 3.5 %copy-start.2 = (bf16[512,512]{1,0:T(8,128)(2,1)S(1)}, bf16[512,512]{1,0:T(8,128)(2,1)}, u32[]{:S(2)}) copy-start(bf16[512,512]{1,0:T(8,128)(2,1)} %copy-done.1) | copy-start | bytes 1572868
  113.5 3.5 %copy-start.25 = (f32[512]{0:T(512)S(1)}, f32[512]{0:T(512)}, u32[]{:S(2)}) copy-start(f32[512]{0:T(512)} %mul.510) | copy-start | bytes 6148
  124.2 1.2 copy-start.7
where the time goes:
time: 127 us; the launch traced here: 126 us
  blocking collectives  30.3 us (24%)
  local copies, waits for them, and re-layouts  28.8 us (23%)
  matrix products  22.6 us (18%)
  other arithmetic  20.4 us (16%)
  starting transfers between devices  19.8 us (16%)
  waiting for transfers between devices  3.3 us (3%)
    ppermute x3, starting transfers between devices, passed_along(): return lax.ppermute(block, axis, route)  12.8 us
    dot_general x8, matrix products, project(): jnp.dot(operand, weights, preferred_element_type=jnp.float32)  12.6 us
    psum x1, blocking collectives, on_device(): reading = lax.psum(partial_value, 'sp')  12.2 us
    psum x1, blocking collectives, from_root(): return lax.psum(kept, axis)  10.5 us
    all_gather x1, blocking collectives, on_device(): lax.all_gather(shard_fading_factor[None], 'sp', axis=0, tiled=True)  7.58 us
    unnamed x75, local copies, waits for them, and re-layouts  6.63 us
    reshape x2, local copies, waits for them, and re-layouts, on_device(): (inner_part + carried_part).reshape(row_count, head_count, HEAD)  5.28 us
    all_to_all x1, starting transfers between devices, on_device(): lax.all_to_all(running[None], 'sp', split_axis=1, concat_axis=0, tiled=True)  3.58 us
  transfers between devices with their start and end apart: 5, of which 1 were waited for; matrix products, arithmetic and copies ran while one was open for 26% of the time, Pallas kernels for 0%

commit v1 on v0

--- a/solution.py
+++ b/solution.py
@@ -8,6 +8,7 @@
 CONV = 4
 BLOCK = 128
 epsilon = 1e-06
+list_the_teams = lambda local_values, ax_name: jax.lax.all_gather(local_values, ax_name).sum(axis=0)
 
 
 def passed_along(block, axis, distance):
@@ -18,7 +19,7 @@
 
 def from_root(value, axis, source):
     kept = jnp.where(lax.axis_index(axis) == source, value, 0).astype(value.dtype)
-    return lax.psum(kept, axis)
+    return list_the_teams(kept, axis)
 
 
 def project(operand, weights):

time: 127 us -> 152 us (1.20)
  blocking collectives: 30.3 us -> 56.9 us
    all_gather x0 -> x3, blocking collectives: none -> 37.1 us  [jax.lax.all_gather(local_values, ax_name).sum(axis=0)]
    psum x1 -> x0, blocking collectives: 10.5 us -> none  [from_root(): return lax.psum(kept, axis)]
    unnamed x0 -> x3, other arithmetic: none -> 1.75 us
    unnamed x75 -> x77, local copies, waits for them, and re-layouts: 6.63 us -> 6.58 us
  transfers between devices with their start and end apart: 5 -> 5, of which waited for: 1 -> 1; matrix products, arithmetic and copies ran while one was open for 26% -> 20% of each run, Pallas kernels for 0% -> 0%
where the time goes in v1:
time: 152 us; the launch traced here: 151 us
  blocking collectives  56.9 us (37%)
  local copies, waits for them, and re-layouts  27.5 us (18%)
  matrix products  22.1 us (15%)
  other arithmetic  20.4 us (13%)
  starting transfers between devices  19.8 us (13%)
  waiting for transfers between devices  3.31 us (2%)
    all_gather x3, blocking collectives, jax.lax.all_gather(local_values, ax_name).sum(axis=0)  37.1 us
    ppermute x3, starting transfers between devices, passed_along(): return lax.ppermute(block, axis, route)  12.8 us
    dot_general x8, matrix products, project(): jnp.dot(operand, weights, preferred_element_type=jnp.float32)  12.6 us
    psum x1, blocking collectives, on_device(): reading = lax.psum(partial_value, 'sp')  12.2 us
    all_gather x1, blocking collectives, on_device(): lax.all_gather(shard_fading_factor[None], 'sp', axis=0, tiled=True)  7.58 us
    unnamed x77, local copies, waits for them, and re-layouts  6.58 us
    reshape x2, local copies, waits for them, and re-layouts, on_device(): (inner_part + carried_part).reshape(row_count, head_count, HEAD)  5.32 us
    all_to_all x1, starting transfers between devices, on_device(): lax.all_to_all(running[None], 'sp', split_axis=1, concat_axis=0, tiled=True)  3.58 us
  transfers between devices with their start and end apart: 5, of which 1 were waited for; matrix products, arithmetic and copies ran while one was open for 20% of the time, Pallas kernels for 0%

profile of v1, /device:TPU:0, one launch (start us, length us, event | category | flops | bytes accessed | tf_op | source)
XLA Modules:
  0.0 151.2 jit_solution(16889777510640651780)
XLA Ops:
  0.7 1.6 %copy-done = bf16[512,2048]{1,0:T(8,128)(2,1)S(1)} copy-done((bf16[512,2048]{1,0:T(8,128)(2,1)S(1)}, bf16[512,2048]{1,0:T(8,128)(2,1)}, u32[]{:S(2)}) %copy-start) | copy-done | bytes 2097176
  2.2 1.9 %convolution_convert_fusion.2 = bf16[512,256]{1,0:T(8,128)(2,1)S(1)} fusion(bf16[512,2048]{1,0:T(8,128)(2,1)S(1)} %copy-done, bf16[2048,256]{1,0:T(8,128)(2,1)} %param.18), kind=kOutput, calls=%fused_computation.11 | convolution fusion | flops 537001984 | bytes 3407872 | tf_op jit(solution)/shard_map/dot_general | solution.py:26
  4.8 5.7 %collective-permute-start.2 = (bf16[3,256]{1,0:T(4,128)(2,1)}, bf16[3,256]{1,0:T(4,128)(2,1)}, u32[]{:S(2)}, u32[]{:S(2)}) collective-permute-start(bf16[3,256]{1,0:T(4,128)(2,1)} %get-tuple-element.54), channel_id=1, source_target_pairs={{0,4},{4,8},{8,12},{1,5},{5,9},{9,13},{2,6},{6,10},{10,14},{3,7},{... | collective-permute-start | bytes 4616 | tf_op jit(solution)/shard_map/ppermute | solution.py:17
  10.4 0.7 convolution_convert_fusion.3
  11.7 3.6 %collective-permute-start.1 = (bf16[3,256]{1,0:T(4,128)(2,1)}, bf16[3,256]{1,0:T(4,128)(2,1)}, u32[]{:S(2)}, u32[]{:S(2)}) collective-permute-start(bf16[3,256]{1,0:T(4,128)(2,1)} %get-tuple-element.52), channel_id=1, source_target_pairs={{0,4},{4,8},{8,12},{1,5},{5,9},{9,13},{2,6},{6,10},{10,14},{3,7},{... | collective-permute-start | bytes 4616 | tf_op jit(solution)/shard_map/ppermute | solution.py:17
  15.3 1.3 convolution_convert_fusion.1
  16.6 0.8 copy-done.8
  18.0 3.5 %collective-permute-start = (bf16[3,512]{1,0:T(4,128)(2,1)}, bf16[3,512]{1,0:T(4,128)(2,1)}, u32[]{:S(2)}, u32[]{:S(2)}) collective-permute-start(bf16[3,512]{1,0:T(4,128)(2,1)} %get-tuple-element.50), channel_id=1, source_target_pairs={{0,4},{4,8},{8,12},{1,5},{5,9},{9,13},{2,6},{6,10},{10,14},{3,7},{... | collective-permute-start | bytes 9224 | tf_op jit(solution)/shard_map/ppermute | solution.py:17
  22.3 1.5 fusion.94
  26.5 2.0 %fusion.97 = f32[1,512]{1,0:T(1,128)S(1)} fusion(bf16[2048,1]{0,1:T(2,128)(2,1)S(1)} %reshape.263, bf16[2048,512]{1,0:T(8,128)(2,1)} %param.20), kind=kOutput, calls=%fused_computation.195 | convolution fusion | flops 2097152 | bytes 2103296 | tf_op jit(solution)/shard_map/dot_general | solution.py:26
  28.5 11.9 %all-gather.6 = bf16[4,3,256]{2,1,0:T(4,128)(2,1)S(1)} all-gather(bf16[1,3,256]{2,1,0:T(4,128)(2,1)S(1)} %get-tuple-element.53), channel_id=4, replica_groups=mesh['grp'=2,'sp'=4,'tp'=4] {'sp'}, dimensions={0}, use_global_device_ids=true | all-gather | bytes 7680 | tf_op jit(solution)/shard_map/all_gather | solution.py:11
  40.5 0.7 convert_convert_fusion
  41.3 11.9 %all-gather.5 = bf16[4,3,256]{2,1,0:T(4,128)(2,1)S(1)} all-gather(bf16[1,3,256]{2,1,0:T(4,128)(2,1)S(1)} %get-tuple-element.51), channel_id=3, replica_groups=mesh['grp'=2,'sp'=4,'tp'=4] {'sp'}, dimensions={0}, use_global_device_ids=true | all-gather | bytes 7680 | tf_op jit(solution)/shard_map/all_gather | solution.py:11
  53.3 7.6 %all-gather.4 = f32[4,2,4]{2,1,0:T(2,128)S(1)} all-gather(f32[1,2,4]{2,1,0:T(2,128)S(1)} %bitcast.158), channel_id=2, replica_groups=mesh['grp'=2,'sp'=4,'tp'=4] {'sp'}, dimensions={0}, use_global_device_ids=true | all-gather | bytes 160 | tf_op jit(solution)/shard_map/all_gather | solution.py:133
  60.9 13.2 %all-gather.7 = bf16[4,3,512]{2,1,0:T(4,128)(2,1)S(1)} all-gather(bf16[1,3,512]{2,1,0:T(4,128)(2,1)S(1)} %get-tuple-element.49), channel_id=5, replica_groups=mesh['grp'=2,'sp'=4,'tp'=4] {'sp'}, dimensions={0}, use_global_device_ids=true | all-gather | bytes 15360 | tf_op jit(solution)/shard_map/all_gather | solution.py:11
  74.1 1.0 copy.149
  75.3 0.7 convert_reduce_fusion.1
  75.9 2.4 %fusion.90 = (f32[4,128,2,4]{3,2,1,0:T(2,128)}, f32[4,128,2,4]{3,2,1,0:T(2,128)S(1)}) fusion(f32[4,128,2,4]{3,2,1,0:T(2,128)S(1)} %fusion.92, f32[4,128,2,4]{3,2,1,0:T(2,128)} %copy.149, f32[4,2,4]{2,1,0:T(2,128)S(1)} %get-tuple-element.44), kind=kLoop, calls=%fused_computation.187 | loop fusion | flops 8192 | bytes 65664 | tf_op jit(solution)/shard_map/exp | solution.py:165
  82.3 1.3 copy.148
  84.4 0.7 maximum_convert_fusion.1
  85.1 1.0 multiply_convert_fusion.6
  86.2 0.8 maximum_convert_fusion.2
  87.5 0.8 maximum_convert_fusion
  88.3 1.3 multiply_convert_fusion.4
  89.7 1.0 copy.140
  90.7 2.0 %reshape.229 = bf16[4,128,2,4,64]{1,0,4,3,2:T(4,128)(2,1)} reshape(bf16[512,512]{0,1:T(8,128)(2,1)} %copy.140) | data formatting | bytes 1048576 | tf_op jit(solution)/shard_map/reshape | solution.py:110
  92.7 1.3 multiply_convert_fusion.3
  94.3 1.0 slice_add_fusion
  95.5 1.2 reshape.286
  96.7 3.6 %all-to-all-start = ((f32[4,1,16384]{2,1,0:T(1,128)}), f32[4,1,16384]{2,1,0:T(1,128)S(1)}, u32[]{:S(2)}, u32[]{:S(2)}) async-start(f32[4,1,16384]{2,1,0:T(1,128)} %reshape.286), calls=%async_computation | async-start | bytes 524288 | tf_op jit(solution)/shard_map/all_to_all | solution.py:137
  100.6 2.9 %convolution_bitcast_fusion.2 = f32[4,128,2,4,64]{1,4,3,2,0:T(8,128)} fusion(f32[4,2,4,128]{3,2,1,0:T(4,128)S(1)} %copy.146, f32[4,2,4,128]{3,2,1,0:T(4,128)S(1)} %copy.144, f32[4,2,128,128]{3,2,1,0:T(8,128)S(1)} %fusion.40, pred[128,128]{1,0:T(8,128)(4,1)S(1)} %iota_compare_fusion, bf16[4,128,2,4,64]{1,0,4,3,2:T(4,128)(2,1)} %reshape.229), kind=kOutput, calls=%fused_computation.5 | convolution fusion | flops 69730304 | bytes 2146304 | tf_op jit(solution)/shard_map/bgels,bsgep->blgep/dot_general | solution.py:161
  103.6 3.3 %all-to-all-done = f32[4,1,16384]{2,1,0:T(1,128)S(1)} async-done(((f32[4,1,16384]{2,1,0:T(1,128)}), f32[4,1,16384]{2,1,0:T(1,128)S(1)}, u32[]{:S(2)}, u32[]{:S(2)}) %all-to-all-start) | async-done | bytes 262176 | tf_op jit(solution)/shard_map/all_to_all | solution.py:137
  107.4 1.3 reduce.15
  109.1 1.3 fusion.35
  110.4 1.3 convolution_bitcast_fusion.3
  111.8 1.0 reshape.288
  112.8 3.4 %all-to-all-start.1 = ((f32[4,1,16384]{2,1,0:T(1,128)}), f32[4,1,16384]{2,1,0:T(1,128)S(1)}, u32[]{:S(2)}, u32[]{:S(2)}) async-start(f32[4,1,16384]{2,1,0:T(1,128)} %reshape.288), calls=%async_computation.1 | async-start | bytes 524288 | tf_op jit(solution)/shard_map/all_to_all | solution.py:148
  116.6 12.2 %psum.7 = f32[2,4,64]{2,1,0:T(4,128)S(1)} all-reduce(f32[2,4,64]{2,1,0:T(4,128)S(1)} %bitcast.143), channel_id=1, replica_groups=mesh['grp'=2,'sp'=4,'tp'=4] {'sp'}, use_global_device_ids=true, to_apply=%region_8.9 | all-reduce | flops 512 | bytes 4096 | tf_op jit(solution)/shard_map/psum | solution.py:201
  129.2 0.7 convert_element_type.217
  130.0 0.8 multiply_convert_fusion.7
  131.6 1.3 reduce.16
  133.2 0.9 copy.160
  134.1 2.3 %fusion.1 = f32[4,128,2,4,64]{1,4,3,2,0:T(8,128)S(1)} fusion(f32[4,128,2,4,64]{1,4,3,2,0:T(8,128)} %convolution_bitcast_fusion.2, f32[1,128,2,4,64]{1,4,3,2,0:T(8,128)} %get-tuple-element.38, f32[1,128,2,4,64]{1,4,3,2,0:T(8,128)} %get-tuple-element.39, f32[1,128,2,4,64]{1,4,3,2,0:T(8,128)} %get-tuple-element.40, f32[4]{0:T(128)S(1)} %copy-done.31, ...), kind=kOutput, calls=%fused_computation.4 | convolution fusion | flops 404488192 | bytes 3424400 | tf_op jit(solution)/shard_map/blgn,bngep->blgep/dot_general | solution.py:165
  136.5 1.8 %copy.184 = f32[4,128,2,4,64]{4,3,2,1,0:T(4,128)} copy(f32[4,128,2,4,64]{1,4,3,2,0:T(8,128)S(1)} %fusion.1) | data formatting | bytes 2097152 | tf_op jit(solution)/shard_map/reshape | solution.py:171
  138.2 3.5 %reshape.275 = f32[512,512]{1,0:T(8,128)} reshape(f32[4,128,2,4,64]{4,3,2,1,0:T(4,128)} %copy.184) | data formatting | bytes 2097152 | tf_op jit(solution)/shard_map/reshape | solution.py:171
  141.8 4.6 %fusion.91 = (f32[512,512]{1,0:T(8,128)}, f32[512,512]{1,0:T(8,128)}) fusion(bf16[512,2048]{1,0:T(8,128)(2,1)S(1)} %copy-done, bf16[2048,512]{1,0:T(8,128)(2,1)} %param.20, f32[512,512]{1,0:T(8,128)} %reshape.275, bf16[512,512]{1,0:T(8,128)(2,1)S(1)} %copy-done.2, f32[512]{0:T(512)S(1)} %copy-done.25), kind=kOutput, calls=%fused_computation.188 | convolution fusion | flops 1076625408 | bytes 7866368 | tf_op jit(solution)/shard_map/dot_general | solution.py:26
  146.4 1.9 %mul.516 = f32[512,2,256]{2,1,0:T(2,128)S(1)} reshape(f32[512,512]{1,0:T(8,128)} %get-tuple-element.60) | data formatting | bytes 2097152 | tf_op jit(solution)/shard_map/mul | solution.py:40
  150.1 1.1 multiply_convert_fusion.2
  (152 shorter events, 16.3 us)
Async XLA Ops:
  0.6 1.6 %copy-start = (bf16[512,2048]{1,0:T(8,128)(2,1)S(1)}, bf16[512,2048]{1,0:T(8,128)(2,1)}, u32[]{:S(2)}) copy-start(bf16[512,2048]{1,0:T(8,128)(2,1)} %param.15) | copy-start | bytes 6291460
  0.6 9.8 %copy-start.6 = (bf16[2048,256]{1,0:T(8,128)(2,1)S(1)}, bf16[2048,256]{1,0:T(8,128)(2,1)}, u32[]{:S(2)}) copy-start(bf16[2048,256]{1,0:T(8,128)(2,1)} %param.19) | copy-start | bytes 3145732
  4.2 7.6 %copy-start.10 = (bf16[512,256]{1,0:T(8,128)(2,1)}, bf16[512,256]{1,0:T(8,128)(2,1)S(1)}, u32[]{:S(2)}) copy-start(bf16[512,256]{1,0:T(8,128)(2,1)S(1)} %convolution_convert_fusion.2) | copy-start | bytes 786436
  4.2 11.2 %copy-start.3 = (bf16[2048,512]{1,0:T(8,128)(2,1)S(1)}, bf16[2048,512]{1,0:T(8,128)(2,1)}, u32[]{:S(2)}) copy-start(bf16[2048,512]{1,0:T(8,128)(2,1)} %param.17) | copy-start | bytes 6291460
  4.8 81.4 %collective-permute-start.2 = (bf16[3,256]{1,0:T(4,128)(2,1)}, bf16[3,256]{1,0:T(4,128)(2,1)}, u32[]{:S(2)}, u32[]{:S(2)}) collective-permute-start(bf16[3,256]{1,0:T(4,128)(2,1)} %get-tuple-element.54), channel_id=1, source_target_pairs={{0,4},{4,8},{8,12},{1,5},{5,9},{9,13},{2,6},{6,10},{10,14},{3,7},{... | collective-permute-start | bytes 4616 | tf_op jit(solution)/shard_map/ppermute | solution.py:17
  11.7 10.3 %copy-start.23 = (bf16[2048]{0:T(1024)(128)(2,1)S(1)}, bf16[2048]{0:T(1024)(128)(2,1)}, u32[]{:S(2)}) copy-start(bf16[2048]{0:T(1024)(128)(2,1)} %param.16) | copy-start | bytes 12292
  11.7 10.3 %copy-start.5 = (bf16[2048,256]{1,0:T(8,128)(2,1)S(1)}, bf16[2048,256]{1,0:T(8,128)(2,1)}, u32[]{:S(2)}) copy-start(bf16[2048,256]{1,0:T(8,128)(2,1)} %param.18) | copy-start | bytes 3145732
  11.7 72.7 %collective-permute-start.1 = (bf16[3,256]{1,0:T(4,128)(2,1)}, bf16[3,256]{1,0:T(4,128)(2,1)}, u32[]{:S(2)}, u32[]{:S(2)}) collective-permute-start(bf16[3,256]{1,0:T(4,128)(2,1)} %get-tuple-element.52), channel_id=1, source_target_pairs={{0,4},{4,8},{8,12},{1,5},{5,9},{9,13},{2,6},{6,10},{10,14},{3,7},{... | collective-permute-start | bytes 4616 | tf_op jit(solution)/shard_map/ppermute | solution.py:17
  16.6 0.8 copy-start.8
  18.0 69.5 %collective-permute-start = (bf16[3,512]{1,0:T(4,128)(2,1)}, bf16[3,512]{1,0:T(4,128)(2,1)}, u32[]{:S(2)}, u32[]{:S(2)}) collective-permute-start(bf16[3,512]{1,0:T(4,128)(2,1)} %get-tuple-element.50), channel_id=1, source_target_pairs={{0,4},{4,8},{8,12},{1,5},{5,9},{9,13},{2,6},{6,10},{10,14},{3,7},{... | collective-permute-start | bytes 9224 | tf_op jit(solution)/shard_map/ppermute | solution.py:17
  21.5 2.3 %copy-start.4 = (bf16[2048,512]{1,0:T(8,128)(2,1)S(1)}, bf16[2048,512]{1,0:T(8,128)(2,1)}, u32[]{:S(2)}) copy-start(bf16[2048,512]{1,0:T(8,128)(2,1)} %param.17) | copy-start | bytes 6291460
  22.0 2.2 %copy-start.33 = (f32[32]{0:T(128)S(1)}, f32[32]{0:T(128)}, u32[]{:S(2)}) copy-start(f32[32]{0:T(128)} %param.26) | copy-start | bytes 388
  22.1 2.3 %copy-start.32 = (f32[32]{0:T(128)S(1)}, f32[32]{0:T(128)}, u32[]{:S(2)}) copy-start(f32[32]{0:T(128)} %param.25) | copy-start | bytes 388
  22.1 2.4 %copy-start.12 = (f32[512,8]{0,1:T(8,128)S(1)}, f32[512,8]{0,1:T(8,128)}, u32[]{:S(2)}) copy-start(f32[512,8]{0,1:T(8,128)} %param.27) | copy-start | bytes 49156
  22.3 2.0 %copy-start.13 = (bf16[2048,32]{0,1:T(8,128)(2,1)S(1)}, bf16[2048,32]{0,1:T(8,128)(2,1)}, u32[]{:S(2)}) copy-start(bf16[2048,32]{0,1:T(8,128)(2,1)} %param.21) | copy-start | bytes 393220
  25.2 15.3 %copy-start.26 = (bf16[4,1024]{1,0:T(4,128)(2,1)S(1)}, bf16[4,1024]{1,0:T(4,128)(2,1)}, u32[]{:S(2)}) copy-start(bf16[4,1024]{1,0:T(4,128)(2,1)} %param.23) | copy-start | bytes 24580
  25.5 49.8 %copy-start.27 = (bf16[4,1024]{1,0:T(4,128)(2,1)S(1)}, bf16[4,1024]{1,0:T(4,128)(2,1)}, u32[]{:S(2)}) copy-start(bf16[4,1024]{1,0:T(4,128)(2,1)} %param.24) | copy-start | bytes 24580
  26.5 51.9 %copy-start.22 = (bf16[4,2048]{1,0:T(4,128)(2,1)S(1)}, bf16[4,2048]{1,0:T(4,128)(2,1)}, u32[]{:S(2)}) copy-start(bf16[4,2048]{1,0:T(4,128)(2,1)} %param.22) | copy-start | bytes 49156
  26.5 53.2 %copy-start.34 = (f32[32]{0:T(128)S(1)}, f32[32]{0:T(128)}, u32[]{:S(2)}) copy-start(f32[32]{0:T(128)} %param.28) | copy-start | bytes 388
  82.3 3.9 %copy-start.11 = (bf16[512,256]{1,0:T(8,128)(2,1)S(1)}, bf16[512,256]{1,0:T(8,128)(2,1)}, u32[]{:S(2)}) copy-start(bf16[512,256]{1,0:T(8,128)(2,1)} %copy-done.10) | copy-start | bytes 786436
  83.8 3.2 %copy-start.18 = (f32[1,256]{1,0:T(1,128)S(1)}, f32[1,256]{1,0:T(1,128)}, u32[]{:S(2)}) copy-start(f32[1,256]{1,0:T(1,128)} %get-tuple-element.28) | copy-start | bytes 3076
  83.8 3.2 %copy-start.19 = (f32[1,256]{1,0:T(1,128)S(1)}, f32[1,256]{1,0:T(1,128)}, u32[]{:S(2)}) copy-start(f32[1,256]{1,0:T(1,128)} %get-tuple-element.29) | copy-start | bytes 3076
  83.8 3.2 %copy-start.20 = (f32[1,256]{1,0:T(1,128)S(1)}, f32[1,256]{1,0:T(1,128)}, u32[]{:S(2)}) copy-start(f32[1,256]{1,0:T(1,128)} %get-tuple-element.30) | copy-start | bytes 3076
  83.8 3.2 %copy-start.21 = (f32[1,256]{1,0:T(1,128)S(1)}, f32[1,256]{1,0:T(1,128)}, u32[]{:S(2)}) copy-start(f32[1,256]{1,0:T(1,128)} %get-tuple-element.31) | copy-start | bytes 3076
  86.1 1.4 copy-start.9
  89.7 4.6 %copy-start.1 = (bf16[512,512]{1,0:T(8,128)(2,1)}, bf16[512,512]{1,0:T(8,128)(2,1)S(1)}, u32[]{:S(2)}) copy-start(bf16[512,512]{1,0:T(8,128)(2,1)S(1)} %multiply_convert_fusion.4) | copy-start | bytes 1572868
  90.7 3.6 %copy-start.14 = (f32[2,4]{1,0:T(2,128)S(1)}, f32[2,4]{1,0:T(2,128)}, u32[]{:S(2)}) copy-start(f32[2,4]{1,0:T(2,128)} %get-tuple-element.45) | copy-start | bytes 100
  90.7 3.6 %copy-start.15 = (f32[2,4]{1,0:T(2,128)S(1)}, f32[2,4]{1,0:T(2,128)}, u32[]{:S(2)}) copy-start(f32[2,4]{1,0:T(2,128)} %get-tuple-element.46) | copy-start | bytes 100
  92.7 1.6 %copy-start.16 = (f32[2,4]{1,0:T(2,128)S(1)}, f32[2,4]{1,0:T(2,128)}, u32[]{:S(2)}) copy-start(f32[2,4]{1,0:T(2,128)} %get-tuple-element.47) | copy-start | bytes 100
  92.7 1.6 %copy-start.17 = (f32[2,4]{1,0:T(2,128)S(1)}, f32[2,4]{1,0:T(2,128)}, u32[]{:S(2)}) copy-start(f32[2,4]{1,0:T(2,128)} %get-tuple-element.48) | copy-start | bytes 100
  96.7 10.2 %all-to-all-start = ((f32[4,1,16384]{2,1,0:T(1,128)}), f32[4,1,16384]{2,1,0:T(1,128)S(1)}, u32[]{:S(2)}, u32[]{:S(2)}) async-start(f32[4,1,16384]{2,1,0:T(1,128)} %reshape.286), calls=%async_computation | async-start | bytes 524288 | tf_op jit(solution)/shard_map/all_to_all | solution.py:137
  100.6 9.8 %copy-start.30 = (pred[4,4]{1,0:T(4,128)(4,1)S(1)}, pred[4,4]{1,0:T(4,128)(4,1)}, u32[]{:S(2)}) copy-start(pred[4,4]{1,0:T(4,128)(4,1)} %iota_compare_fusion.1) | copy-start | bytes 52
  109.0 7.2 %copy-start.28 = (f32[2,4]{1,0:T(2,128)S(1)}, f32[2,4]{1,0:T(2,128)}, u32[]{:S(2)}) copy-start(f32[2,4]{1,0:T(2,128)} %mul.529) | copy-start | bytes 100
  109.0 7.4 %copy-start.24 = (bf16[2,32,1,1]{1,0,2,3:T(2,128)(2,1)S(1)}, bf16[2,32,1,1]{1,0,2,3:T(2,128)(2,1)}, u32[]{:S(2)}) copy-start(bf16[2,32,1,1]{1,0,2,3:T(2,128)(2,1)} %fusion.81) | copy-start | bytes 388
  110.4 18.4 %copy-start.29 = (f32[2,4]{1,0:T(2,128)S(1)}, f32[2,4]{1,0:T(2,128)}, u32[]{:S(2)}) copy-start(f32[2,4]{1,0:T(2,128)} %mul.552) | copy-start | bytes 100
  112.8 18.8 %all-to-all-start.1 = ((f32[4,1,16384]{2,1,0:T(1,128)}), f32[4,1,16384]{2,1,0:T(1,128)S(1)}, u32[]{:S(2)}, u32[]{:S(2)}) async-start(f32[4,1,16384]{2,1,0:T(1,128)} %reshape.288), calls=%async_computation.1 | async-start | bytes 524288 | tf_op jit(solution)/shard_map/all_to_all | solution.py:148
  116.3 17.9 %copy-start.31 = (f32[4]{0:T(128)S(1)}, f32[4]{0:T(128)}, u32[]{:S(2)}) copy-start(f32[4]{0:T(128)} %pad.6.clone) | copy-start | bytes 52
  138.2 3.5 %copy-start.2 = (bf16[512,512]{1,0:T(8,128)(2,1)S(1)}, bf16[512,512]{1,0:T(8,128)(2,1)}, u32[]{:S(2)}) copy-start(bf16[512,512]{1,0:T(8,128)(2,1)} %copy-done.1) | copy-start | bytes 1572868
  138.2 3.5 %copy-start.25 = (f32[512]{0:T(512)S(1)}, f32[512]{0:T(512)}, u32[]{:S(2)}) copy-start(f32[512]{0:T(512)} %mul.510) | copy-start | bytes 6148
  148.9 1.2 copy-start.7
